TPU v7x, 256 devices: a 2x2x32 block of a 4x8x32 slice. The times are simulated.
256 devices in a mesh: grp: 4 (over y, x), ep: 64 (over z, core).
Axes of the slice: x: 2, y: 2, z: 32, core: 2. Of those that a mesh axis runs over, the one named last changes fastest.
The devices are a block of a 4x8x32 slice.
Arguments:
- tokens: bfloat16 [8192, 2048], P(('grp', 'ep')), parts along dimension 0, may hold values from -6 to 6
- norm_gain: float32 [2048], replicated, may hold values from 0.1 to 1.9
- routing: int32 [8192, 8], P(('grp', 'ep')), parts along dimension 0, may hold values from 0 to 63, all different within a row; in each aligned block of 32 rows (0 to 31, 32 to 63, ...) at most 8 rows name the same one
- gates: float32 [8192, 8], P(('grp', 'ep')), parts along dimension 0, may hold values from 0.05 to 0.6
- w_gate: bfloat16 [64, 2048, 512], P('ep'), may hold values from -0.125 to 0.125
- w_up: bfloat16 [64, 2048, 512], P('ep'), may hold values from -0.125 to 0.125
- w_down: bfloat16 [64, 512, 2048], P('ep'), may hold values from -0.25 to 0.25
- shared_gate: bfloat16 [2048, 512], replicated, may hold values from -0.125 to 0.125
- shared_up: bfloat16 [2048, 512], replicated, may hold values from -0.125 to 0.125
- shared_down: bfloat16 [512, 2048], replicated, may hold values from -0.25 to 0.25
Outputs:
- mixed: bfloat16 [8192, 2048], P(('grp', 'ep')), parts along dimension 0
There are 4 independent parts, one for each index of `grp`. A program takes and returns all parts, laid end to end along the dimension named above; an argument that names none is the same for every part. Nothing has to cross between parts.
Inputs may be any that keep to these rules, and one draw needn't show every extreme that they name: `routing`: within the 32 rows of one device no expert is named by more than 8 rows, and in every draw some expert is named by exactly 8 rows of some device; each row names 8 different experts.
All inputs are finite; a program needn't handle non-finite values.
Results may differ from a plain program's by a relative error of at most 0.0067.
Values may be sent and summed in bfloat16 or wider, within the bound.
A program may use at most 128 MiB of HBM per device.

v0:
```python
import jax
import jax.numpy as jnp
from jax import lax
from jax.sharding import PartitionSpec as P

epsilon = 1e-06


def rms_normed(tokens, norm_gain):
    floats = tokens.astype(jnp.float32)
    scale_inv = lax.rsqrt(jnp.mean(floats * floats, axis=-1, keepdims=True) + epsilon)
    return (floats * scale_inv * norm_gain).astype(jnp.bfloat16)


def expert_outputs(buffer, w_gate, w_up, w_down):
    gate_act = jnp.einsum("nesd,edf->nesf", buffer, w_gate, preferred_element_type=jnp.float32)
    up_act = jnp.einsum("nesd,edf->nesf", buffer, w_up, preferred_element_type=jnp.float32)
    hidden = (jax.nn.silu(gate_act) * up_act).astype(jnp.bfloat16)
    return jnp.einsum("nesf,efd->nesd", hidden, w_down, preferred_element_type=jnp.float32).astype(
        jnp.bfloat16
    )


def slot_targets(routing, expert_count, slot_count):
    leading = routing.shape[:-2]
    tok_count, top_count = routing.shape[-2:]
    flattened = routing.reshape(leading + (tok_count * top_count,))
    onehot = (flattened[..., None] == jnp.arange(expert_count, dtype=jnp.int32)).astype(jnp.int32)
    earlier = jnp.cumsum(onehot, axis=-2) - onehot
    within = jnp.sum(earlier * onehot, axis=-1)
    return (flattened * slot_count + within).reshape(routing.shape)


def slot_tables(targets, gates, row_count):
    slot_ids = jnp.arange(row_count, dtype=jnp.int32)
    matches = targets[..., None] == slot_ids
    selected = jnp.any(matches, axis=-2)
    weights = jnp.sum(
        jnp.where(matches, gates[..., None], jnp.zeros_like(gates[..., None])), axis=-2
    )
    return (selected, weights)


def body(
    tokens, norm_gain, routing, gates, w_gate, w_up, w_down, shared_gate, shared_up, shared_down
):
    normed = rms_normed(tokens, norm_gain)
    shared_hidden = (
        jax.nn.silu(jnp.dot(normed, shared_gate, preferred_element_type=jnp.float32))
        * jnp.dot(normed, shared_up, preferred_element_type=jnp.float32)
    ).astype(jnp.bfloat16)
    shared_out = jnp.dot(shared_hidden, shared_down, preferred_element_type=jnp.float32)
    tok_count, top_count = routing.shape
    local_count = w_gate.shape[0]
    ep_size = lax.axis_size("ep")
    expert_count = local_count * ep_size
    slot_count = max(4, (2 * tok_count * top_count + expert_count - 1) // expert_count)
    model_width = normed.shape[1]
    targets = slot_targets(routing, expert_count, slot_count)
    selected, weights = slot_tables(targets, gates, expert_count * slot_count)
    buffer = jnp.einsum(
        "tr,td->rd", selected.astype(jnp.bfloat16), normed, preferred_element_type=jnp.float32
    ).astype(jnp.bfloat16)
    buffer = buffer.reshape(ep_size, local_count, slot_count, model_width)
    returned = lax.all_to_all(
        expert_outputs(
            lax.all_to_all(buffer, "ep", split_axis=0, concat_axis=0, tiled=True),
            w_gate,
            w_up,
            w_down,
        ),
        "ep",
        split_axis=0,
        concat_axis=0,
        tiled=True,
    )
    returned = returned.reshape(expert_count * slot_count, model_width)
    chosen_rows = returned[targets.reshape(-1)].reshape(tok_count, top_count, model_width)
    routed = jnp.sum(gates[..., None] * chosen_rows.astype(jnp.float32), axis=1)
    return (shared_out + routed).astype(jnp.bfloat16)


def solution(mesh):
    placed = (
        P(("grp", "ep"), None),
        P(),
        P(("grp", "ep"), None),
        P(("grp", "ep"), None),
        P("ep", None, None),
        P("ep", None, None),
        P("ep", None, None),
        P(),
        P(),
        P(),
    )
    return jax.shard_map(
        body, mesh=mesh, in_specs=placed, out_specs=P(("grp", "ep"), None), check_vma=False
    )
```

profile of v0, /device:TPU:37, one launch (start us, length us, event | category | flops | bytes accessed | tf_op | source)
XLA Modules:
  0.0 462.0 jit_solution(6392350227190849025)
XLA Ops:
  0.0 0.0 copy-start
  0.0 0.9 copy.26
  0.9 0.1 eq.42
  1.0 0.1 eq.38
  1.1 0.6 reduce-window.6
  1.7 0.2 slice_reduce_fusion
  1.9 0.1 fusion.48
  2.1 0.1 reduce_sum.33
  2.2 0.2 fusion.42
  2.4 1.0 fusion.43
  3.5 1.7 fusion
  5.1 0.0 copy-start.5
  5.2 231.6 %all_to_all.10 = bf16[64,1,8,2048]{3,2,1,0:T(8,128)(2,1)S(1)} all-to-all(bf16[64,1,8,2048]{3,2,1,0:T(8,128)(2,1)S(1)} %fusion), channel_id=1, replica_groups=mesh['grp'=4,'ep'=64] {'ep'}, dimensions={0} | all-to-all | bytes 4194304 | tf_op jit(solution)/shard_map/all_to_all | solution.py:67
  236.8 0.0 copy-start.2
  236.8 1.3 copy-done.2
  238.1 0.0 copy-done.5
  238.1 1.2 fusion.11
  239.3 0.0 copy-done
  239.3 6.0 %fusion.1 = bf16[64,1,8,2048]{3,2,1,0:T(8,128)(2,1)} fusion(bf16[1,512,2048]{2,1,0:T(8,128)(2,1)S(1)} %copy-done, bf16[1,2048,512]{2,1,0:T(8,128)(2,1)} %param.15, bf16[64,1,8,2048]{3,2,1,0:T(8,128)(2,1)} %copy-done.2, f32[64,1,8,512]{3,2,0,1:T(8,128)S(1)} %fusion.11), kind=kOutput, calls=%fused_computation.4 | convolution fusion | flops 2150105088 | bytes 9437184 | tf_op jit(solution)/shard_map/nesf,efd->nesd/dot_general | solution.py:19
  245.3 0.0 copy-start.4
  245.3 0.0 copy-start.1
  245.3 8.7 %all-to-all-start.1 = ((bf16[64,1,8,2048]{3,2,1,0:T(8,128)(2,1)}), bf16[64,1,8,2048]{3,2,1,0:T(8,128)(2,1)}, u32[]{:S(2)}, u32[]{:S(2)}) async-start(bf16[64,1,8,2048]{3,2,1,0:T(8,128)(2,1)} %fusion.1), calls=%async_computation.1 | async-start | bytes 4194304 | tf_op jit(solution)/shard_map/all_to_all | solution.py:65
  254.0 0.1 mul.75
  254.1 0.0 copy-done.4
  254.1 0.7 copy.25
  254.8 0.0 copy-done.1
  254.8 0.0 copy-done.3
  254.8 2.7 fusion.62
  257.5 194.7 %all-to-all-done.1 = bf16[64,1,8,2048]{3,2,1,0:T(8,128)(2,1)} async-done(((bf16[64,1,8,2048]{3,2,1,0:T(8,128)(2,1)}), bf16[64,1,8,2048]{3,2,1,0:T(8,128)(2,1)}, u32[]{:S(2)}, u32[]{:S(2)}) %all-to-all-start.1) | async-done | bytes 2097184 | tf_op jit(solution)/shard_map/all_to_all | solution.py:65
  452.2 4.2 gather_fusion
  456.5 1.7 fusion.3
  458.2 3.9 fusion.2
  (8 shorter events, 0.1 us)
Async XLA Ops:
  0.0 239.3 %copy-start = (bf16[1,512,2048]{2,1,0:T(8,128)(2,1)S(1)}, bf16[1,512,2048]{2,1,0:T(8,128)(2,1)}, u32[]{:S(2)}) copy-start(bf16[1,512,2048]{2,1,0:T(8,128)(2,1)} %param.16) | copy-start | bytes 6291460
  5.1 232.9 %copy-start.5 = (bf16[1,2048,512]{2,1,0:T(8,128)(2,1)S(1)}, bf16[1,2048,512]{2,1,0:T(8,128)(2,1)}, u32[]{:S(2)}) copy-start(bf16[1,2048,512]{2,1,0:T(8,128)(2,1)} %param.14) | copy-start | bytes 6291460
  236.8 1.3 copy-start.2
  245.3 8.8 %copy-start.4 = (f32[32,8]{0,1:T(8,128)S(1)}, f32[32,8]{0,1:T(8,128)}, u32[]{:S(2)}) copy-start(f32[32,8]{0,1:T(8,128)} %param.13) | copy-start | bytes 3076
  245.3 9.5 %copy-start.1 = (bf16[32,2048]{1,0:T(8,128)(2,1)S(1)}, bf16[32,2048]{1,0:T(8,128)(2,1)}, u32[]{:S(2)}) copy-start(bf16[32,2048]{1,0:T(8,128)(2,1)} %param.10) | copy-start | bytes 393220
  245.3 9.5 %copy-start.3 = (f32[2048]{0:T(1024)S(1)}, f32[2048]{0:T(1024)}, u32[]{:S(2)}) copy-start(f32[2048]{0:T(1024)} %param.11) | copy-start | bytes 24580
  245.3 206.9 %all-to-all-start.1 = ((bf16[64,1,8,2048]{3,2,1,0:T(8,128)(2,1)}), bf16[64,1,8,2048]{3,2,1,0:T(8,128)(2,1)}, u32[]{:S(2)}, u32[]{:S(2)}) async-start(bf16[64,1,8,2048]{3,2,1,0:T(8,128)(2,1)} %fusion.1), calls=%async_computation.1 | async-start | bytes 4194304 | tf_op jit(solution)/shard_map/all_to_all | solution.py:65
where the time goes:
time: 464 us; the launch traced here: 462 us
  blocking collectives  232 us (50%)
  waiting for transfers between devices  195 us (42%)
  matrix products  15.5 us (3%)
  starting transfers between devices  8.65 us (2%)
  local copies, waits for them, and re-layouts  7.66 us (2%)
    all_to_all x1, blocking collectives, body(): lax.all_to_all(buffer, 'ep', split_axis=0, concat_axis=0, tiled=True)  232 us
    all_to_all x1, waiting for transfers between devices, body(): lax.all_to_all(expert_outputs(lax.all_to_all(buffer, 'ep', split_axis=0,...  195 us
  transfers between devices with their start and end apart: 1, of which 1 were waited for; matrix products, arithmetic and copies ran while one was open for 1% of the time, Pallas kernels for 0%

commit v1 on v0

v1 whole, which is shorter than its diff:
```python
import jax
import jax.numpy as jnp
from jax import lax
from jax.sharding import PartitionSpec as P

epsilon = 1e-06


def rms_normed(tokens, norm_gain):
    floats = tokens.astype(jnp.float32)
    scale_inv = lax.rsqrt(jnp.mean(floats * floats, axis=-1, keepdims=True) + epsilon)
    return (floats * scale_inv * norm_gain).astype(jnp.bfloat16)


def body(
    tokens, norm_gain, routing, gates, w_gate, w_up, w_down, shared_gate, shared_up, shared_down
):
    normed = rms_normed(tokens, norm_gain)
    shared_hidden = (
        jax.nn.silu(jnp.dot(normed, shared_gate, preferred_element_type=jnp.float32))
        * jnp.dot(normed, shared_up, preferred_element_type=jnp.float32)
    ).astype(jnp.bfloat16)
    shared_out = jnp.dot(shared_hidden, shared_down, preferred_element_type=jnp.float32)
    everyone = lax.all_gather(normed, "ep", axis=0, tiled=True)
    routes = lax.all_gather(routing, "ep", axis=0, tiled=True)
    weights = lax.all_gather(gates, "ep", axis=0, tiled=True)
    own = lax.axis_index("ep")
    scale = jnp.sum(jnp.where(routes == own, weights, 0.0), axis=-1, keepdims=True)
    hidden = (
        jax.nn.silu(jnp.dot(everyone, w_gate[0], preferred_element_type=jnp.float32))
        * jnp.dot(everyone, w_up[0], preferred_element_type=jnp.float32)
    ) * scale
    part = jnp.dot(
        hidden.astype(jnp.bfloat16), w_down[0], preferred_element_type=jnp.float32
    ).astype(jnp.bfloat16)
    routed = lax.psum_scatter(part, "ep", scatter_dimension=0, tiled=True)
    return (shared_out + routed.astype(jnp.float32)).astype(jnp.bfloat16)


def solution(mesh):
    placed = (
        P(("grp", "ep"), None),
        P(),
        P(("grp", "ep"), None),
        P(("grp", "ep"), None),
        P("ep", None, None),
        P("ep", None, None),
        P("ep", None, None),
        P(),
        P(),
        P(),
    )
    return jax.shard_map(
        body, mesh=mesh, in_specs=placed, out_specs=P(("grp", "ep"), None), check_vma=False
    )
```

time: 464 us -> 402 us (0.87)
  blocking collectives: 232 us -> 131 us
  waiting for transfers between devices: 195 us -> 227 us
  between operations: 0.12 us -> 13.5 us
  matrix products: 15.5 us -> 25.5 us
  starting transfers between devices: 8.65 us -> 0.07 us
  local copies, waits for them, and re-layouts: 7.66 us -> 0.93 us
    all_to_all x1 -> x0, blocking collectives: 232 us -> none  [body(): lax.all_to_all(buffer, 'ep', split_axis=0, concat_axis=0, tiled=True)]
    reduce_scatter x0 -> x1, waiting for transfers between devices: none -> 206 us  [body(): routed = lax.psum_scatter(part, 'ep', scatter_dimension=0, tiled=True)]
    all_to_all x1 -> x0, waiting for transfers between devices: 195 us -> none  [body(): lax.all_to_all(expert_outputs(lax.all_to_all(buffer, 'ep', split_axis=0,...]
    all_gather x0 -> x2, blocking collectives: none -> 131 us  [the longest x1 77.4 us: body(): routes = lax.all_gather(routing, 'ep', axis=0, tiled=True)]
    all_gather x0 -> x1, waiting for transfers between devices: none -> 21 us  [body(): everyone = lax.all_gather(normed, 'ep', axis=0, tiled=True)]
    dot_general x3, matrix products: 8.89 us -> 19.7 us  [the longest x1 7.67 us: body(): jnp.dot(everyone, w_gate[0], preferred_element_type=jnp.float32)]
    all_to_all x1 -> x0, starting transfers between devices: 8.65 us -> none  [body(): lax.all_to_all(expert_outputs(lax.all_to_all(buffer, 'ep', split_axis=0,...]
  transfers between devices with their start and end apart: 1 -> 2, of which waited for: 1 -> 2; matrix products, arithmetic and copies ran while one was open for 1% -> 1% of each run, Pallas kernels for 0% -> 0%
where the time goes in v1:
time: 402 us; the launch traced here: 401 us
  waiting for transfers between devices  227 us (56%)
  blocking collectives  131 us (33%)
  matrix products  25.5 us (6%)
  between operations  13.5 us (3%)
    reduce_scatter x1, waiting for transfers between devices, body(): routed = lax.psum_scatter(part, 'ep', scatter_dimension=0, tiled=True)  206 us
    all_gather x1, blocking collectives, body(): routes = lax.all_gather(routing, 'ep', axis=0, tiled=True)  77.4 us
    all_gather x1, blocking collectives, body(): weights = lax.all_gather(gates, 'ep', axis=0, tiled=True)  53.5 us
    all_gather x1, waiting for transfers between devices, body(): everyone = lax.all_gather(normed, 'ep', axis=0, tiled=True)  21 us
  transfers between devices with their start and end apart: 2, of which 2 were waited for; matrix products, arithmetic and copies ran while one was open for 1% of the time, Pallas kernels for 0%

profile of v1, /device:TPU:37, one launch (start us, length us, event | category | flops | bytes accessed | tf_op | source)
XLA Modules:
  0.0 400.8 jit_solution(2111920116285077826)
XLA Ops:
  6.5 0.0 copy-start
  6.6 0.0 all-gather.4.cloned.1.call-start
  6.6 1.2 fusion.6
  7.7 1.7 fusion.8
  9.4 0.1 all-gather.4.cloned.1.call-update
  9.5 0.1 reduce-scatter.2.cloned.1.call-start
  9.6 77.4 %all-gather = s32[64,32,8]{1,2,0:T(8,128)S(1)} all-gather(s32[1,32,8]{1,2,0:T(8,128)} %bitcast.19), channel_id=1, replica_groups=mesh['grp'=4,'ep'=64] {'ep'}, dimensions={0}, use_global_device_ids=true | all-gather | bytes 66560 | tf_op jit(solution)/shard_map/all_gather | solution.py:25
  86.9 53.5 %all-gather.1 = f32[64,32,8]{1,2,0:T(8,128)S(1)} all-gather(f32[1,32,8]{1,2,0:T(8,128)} %bitcast.20), channel_id=1, replica_groups=mesh['grp'=4,'ep'=64] {'ep'}, dimensions={0}, use_global_device_ids=true | all-gather | bytes 66560 | tf_op jit(solution)/shard_map/all_gather | solution.py:26
  140.4 0.1 select_reduce_fusion
  140.5 0.1 reshape.18
  140.6 21.0 %all-gather.4.cloned.1.call-done = bf16[2048,2048]{1,0:T(8,128)(2,1)} async-done(((bf16[32,2048]{1,0:T(8,128)(2,1)}), bf16[2048,2048]{1,0:T(8,128)(2,1)}) %all-gather.4.cloned.1.call-update) | async-done | bytes 8388624 | tf_op jit(solution)/shard_map/all_gather | solution.py:24
  161.6 0.0 copy-start.2
  161.6 0.0 copy-start.3
  161.6 7.7 %fusion.3 = f32[2048,512]{1,0:T(8,128)S(1)} fusion(bf16[2048,2048]{1,0:T(8,128)(2,1)} %all-gather.4.cloned.1.call-done, bf16[1,2048,512]{2,1,0:T(8,128)(2,1)} %param.14), kind=kOutput, calls=%fused_computation.6 | convolution fusion | flops 4294967296 | bytes 14680064 | tf_op jit(solution)/shard_map/dot_general | solution.py:30
  169.3 0.0 copy-done.2
  169.3 0.0 copy-done.3
  169.3 5.2 %multiply_convert_fusion = bf16[2048,512]{1,0:T(8,128)(2,1)S(1)} fusion(f32[2048,512]{1,0:T(8,128)S(1)} %fusion.3, bf16[2048,2048]{1,0:T(8,128)(2,1)S(1)} %copy-done.2, bf16[1,2048,512]{2,1,0:T(8,128)(2,1)S(1)} %copy-done.3, f32[2048]{0:T(1024)S(1)} %reshape.18), kind=kOutput, calls=%fused_computation.1 | convolution fusion | flops 4302307328 | bytes 16785408 | tf_op jit(solution)/shard_map/dot_general | solution.py:31
  174.5 0.0 copy-done
  174.6 6.8 %convolution_convert_fusion = bf16[2048,2048]{1,0:T(8,128)(2,1)} fusion(bf16[2048,512]{1,0:T(8,128)(2,1)S(1)} %multiply_convert_fusion, bf16[1,512,2048]{2,1,0:T(8,128)(2,1)S(1)} %copy-done), kind=kOutput, calls=%fused_computation | convolution fusion | flops 4299161600 | bytes 12582912 | tf_op jit(solution)/shard_map/dot_general | solution.py:33
  181.3 0.0 copy-start.1
  181.3 0.1 reduce-scatter.2.cloned.1.call-update
  181.4 0.8 copy-done.1
  182.2 2.0 fusion.16
  184.3 205.9 %reduce-scatter.2.cloned.1.call-done = bf16[32,2048]{1,0:T(8,128)(2,1)} async-done(((bf16[2048,2048]{1,0:T(8,128)(2,1)}), bf16[32,2048]{1,0:T(8,128)(2,1)}) %reduce-scatter.2.cloned.1.call-update) | async-done | bytes 131088 | tf_op jit(solution)/shard_map/reduce_scatter | solution.py:36
  390.2 3.8 fusion
  (1 shorter events, 0.0 us)
Async XLA Ops:
  6.5 168.0 %copy-start = (bf16[1,512,2048]{2,1,0:T(8,128)(2,1)S(1)}, bf16[1,512,2048]{2,1,0:T(8,128)(2,1)}, u32[]{:S(2)}) copy-start(bf16[1,512,2048]{2,1,0:T(8,128)(2,1)} %param.16) | copy-start | bytes 6291460
  6.6 155.0 %all-gather.4.cloned.1.call-start = ((), (), s32[]{:S(2)}) async-start(), calls=%async_computation.1 | async-start | bytes 8519680 | tf_op jit(solution)/shard_map/all_gather | solution.py:24
  9.5 380.7 %reduce-scatter.2.cloned.1.call-start = ((), (), s32[]{:S(2)}) async-start(), calls=%async_computation.2 | async-start | bytes 8519680 | tf_op jit(solution)/shard_map/reduce_scatter | solution.py:36
  161.6 7.7 %copy-start.2 = (bf16[2048,2048]{1,0:T(8,128)(2,1)S(1)}, bf16[2048,2048]{1,0:T(8,128)(2,1)}, u32[]{:S(2)}) copy-start(bf16[2048,2048]{1,0:T(8,128)(2,1)} %all-gather.4.cloned.1.call-done) | copy-start | bytes 25165828
  161.6 7.7 %copy-start.3 = (bf16[1,2048,512]{2,1,0:T(8,128)(2,1)S(1)}, bf16[1,2048,512]{2,1,0:T(8,128)(2,1)}, u32[]{:S(2)}) copy-start(bf16[1,2048,512]{2,1,0:T(8,128)(2,1)} %param.15) | copy-start | bytes 6291460
  181.3 0.9 copy-start.1
Sparse Core Ops, SparseCore 0:
  9.6 151.9 all-gather.3
  181.5 208.5 reduce-scatter.1
